TPU v7x, 32 devices: a whole 2x2x4 slice. The times are simulated.
32 devices in a mesh: kv: 8 (over z, y), tp: 4 (over x, core).
Axes of the slice: x: 2, y: 2, z: 4, core: 2. Of those that a mesh axis runs over, the one named last changes fastest.
Arguments:
- tokens: bfloat16 [4, 4096], P(None, ('kv', 'tp')), may hold values from -6 to 6
- gain_first: bfloat16 [4096], P(('kv', 'tp')), may hold values from 0.099609375 to 1.8984375
- w_query: bfloat16 [4096, 2048], P('kv', 'tp'), may hold values from -0.09375 to 0.09375
- w_key: bfloat16 [4096, 2048], P('kv', 'tp'), may hold values from -0.09375 to 0.09375
- w_value: bfloat16 [4096, 2048], P('kv', 'tp'), may hold values from -0.09375 to 0.09375
- w_forget: bfloat16 [4096, 32], P('kv'), may hold values from -0.1875 to 0.1875
- forget_bias: float32 [32], P('tp'), may hold values from 1 to 6
- past_keys: bfloat16 [4, 16384, 2048], P(None, 'kv', 'tp'), may hold values from -48 to 48
- past_values: bfloat16 [4, 16384, 2048], P(None, 'kv', 'tp'), may hold values from -6 to 6
- past_forget: float32 [4, 32, 16384], P(None, 'tp', 'kv'), may hold values from -0.25 to 0, as said below
- w_out: bfloat16 [2048, 4096], P('tp', 'kv'), may hold values from -0.5 to 0.5
- gain_second: bfloat16 [4096], P(('kv', 'tp')), may hold values from 0.099609375 to 1.8984375
- w_gate: bfloat16 [4096, 11264], P(None, ('kv', 'tp')), may hold values from -0.09375 to 0.09375
- w_up: bfloat16 [4096, 11264], P(None, ('kv', 'tp')), may hold values from -0.09375 to 0.09375
- w_down: bfloat16 [11264, 4096], P(('kv', 'tp')), may hold values from -0.109375 to 0.109375
Outputs:
- layer_out: bfloat16 [4, 4096], P(None, ('kv', 'tp'))
- new_keys: bfloat16 [4, 2048], P(None, 'tp')
- new_values: bfloat16 [4, 2048], P(None, 'tp')
- new_forget: float32 [4, 32], P(None, 'tp')
Inputs may be any that keep to these rules, and one draw needn't show every extreme that they name: `past_forget`: each entry is the logarithm of a forget gate: negative, and no smaller than -0.25.
All inputs are finite; a program needn't handle non-finite values.
Results may differ from a plain program's by a relative error of at most 0.0095.
The roundings to bfloat16 on the way count: a program that leaves them out, or rounds other values in their place, can miss the bound.
Values may be sent and summed in bfloat16 or wider, within the bound.
A program may use at most 128 MiB of HBM per device.

v0:
```python
import jax
import jax.numpy as jnp
from jax import lax
from jax.sharding import PartitionSpec as P

epsilon = 1e-05


def prefix(part, axis, combine, identity):
    count = lax.axis_size(axis)
    place = lax.axis_index(axis)
    ahead = count - 1 - place
    gathered = lax.all_gather(part, axis)
    state = jnp.zeros_like(part) + jnp.asarray(identity, part.dtype)

    def one(hop, state):
        source = count - 1 - hop
        return combine(state, lax.dynamic_index_in_dim(gathered, source, 0, False))

    return lax.fori_loop(0, ahead, one, state)


def merged(array, axis, combine):
    everything = jax.tree.map(lambda part: lax.all_gather(part, axis), array)
    initial = jax.tree.map(lambda part: part[0], everything)

    def hop(k, so_far):
        return combine(so_far, jax.tree.map(lambda part: part[k], everything))

    return lax.fori_loop(1, lax.axis_size(axis), hop, initial)


def row_scales(first_sum, second_sum, row_width):
    row_mean = first_sum / row_width
    spread = jnp.maximum(second_sum / row_width - row_mean * row_mean, 0.0) + epsilon
    return (row_mean, lax.rsqrt(spread))


def add_terms(first_term, second_term):
    return first_term + second_term


def combine_blocks(left_part, right_part):
    highest = jnp.maximum(left_part[0], right_part[0])
    left_factor = jnp.exp(left_part[0] - highest)
    right_factor = jnp.exp(right_part[0] - highest)
    totals = left_part[1] * left_factor + right_part[1] * right_factor
    mixtures = left_part[2] * left_factor[..., None] + right_part[2] * right_factor[..., None]
    return (highest, totals, mixtures)


def local(
    tokens,
    gain_first,
    w_query,
    w_key,
    w_value,
    w_forget,
    forget_bias,
    past_keys,
    past_values,
    past_forget,
    w_out,
    gain_second,
    w_gate,
    w_up,
    w_down,
):
    local_rows, local_gain = (
        lax.all_gather(tokens, "tp", axis=1, tiled=True),
        lax.all_gather(gain_first, "tp", axis=0, tiled=True),
    )
    wide_rows = local_rows.astype(jnp.float32)
    scaled = (wide_rows * local_gain.astype(jnp.float32)).astype(jnp.bfloat16)
    heads_here = forget_bias.shape[0]
    forget_cols = lax.dynamic_slice_in_dim(
        w_forget, lax.axis_index("tp") * heads_here, heads_here, 1
    )
    gain_row = local_gain[None, :]
    summed = lax.psum(
        (
            jnp.dot(scaled, w_query, preferred_element_type=jnp.float32),
            jnp.dot(scaled, w_key, preferred_element_type=jnp.float32),
            jnp.dot(scaled, w_value, preferred_element_type=jnp.float32),
            jnp.dot(scaled, forget_cols, preferred_element_type=jnp.float32),
            jnp.dot(gain_row, w_query, preferred_element_type=jnp.float32),
            jnp.dot(gain_row, w_key, preferred_element_type=jnp.float32),
            jnp.dot(gain_row, w_value, preferred_element_type=jnp.float32),
            jnp.dot(gain_row, forget_cols, preferred_element_type=jnp.float32),
            jnp.sum(wide_rows, axis=1),
            jnp.sum(wide_rows * wide_rows, axis=1),
        ),
        "kv",
    )
    row_mean, row_scale = row_scales(
        summed[8][:, None], summed[9][:, None], local_rows.shape[1] * lax.axis_size("kv")
    )

    def finish(member):
        return row_scale * (summed[member] - row_mean * summed[member + 4])

    query = finish(0).astype(jnp.bfloat16)
    new_keys = finish(1).astype(jnp.bfloat16)
    new_values = finish(2).astype(jnp.bfloat16)
    new_forget = jax.nn.log_sigmoid(finish(3) + forget_bias)
    batch_rows = tokens.shape[0]
    head_size = query.shape[1] // heads_here
    span_here = past_keys.shape[1]
    score_scale = head_size ** (-0.5)
    query_heads = query.reshape(batch_rows, heads_here, head_size)
    key_heads = past_keys.reshape(batch_rows, span_here, heads_here, head_size)
    value_heads = past_values.reshape(batch_rows, span_here, heads_here, head_size)
    inclusive = jnp.cumsum(past_forget, axis=2)
    block_total = inclusive[:, :, -1]
    later_sum = prefix(block_total, "kv", add_terms, jnp.zeros_like(block_total))
    decay_bias = (new_forget + later_sum + block_total)[:, :, None] - inclusive
    logits = (
        jnp.einsum("bhd,bshd->bhs", query_heads, key_heads, preferred_element_type=jnp.float32)
        * score_scale
        + decay_bias
    )
    block_top = jnp.max(logits, axis=2)
    weights = jnp.exp(logits - block_top[:, :, None])
    block_sum = jnp.sum(weights, axis=2)
    block_mix = jnp.einsum(
        "bhs,bshd->bhd",
        weights.astype(jnp.bfloat16),
        value_heads,
        preferred_element_type=jnp.float32,
    ).astype(jnp.bfloat16)
    carried = lax.optimization_barrier(block_mix).astype(jnp.float32)
    highest, totals, mixtures = merged((block_top, block_sum, carried), "kv", combine_blocks)
    own_keys = new_keys.reshape(batch_rows, heads_here, head_size)
    own_values = (
        lax.optimization_barrier(new_values)
        .astype(jnp.float32)
        .reshape(batch_rows, heads_here, head_size)
    )
    own_score = (
        jnp.einsum("bhd,bhd->bh", query_heads, own_keys, preferred_element_type=jnp.float32)
        * score_scale
    )
    top_all = jnp.maximum(highest, own_score)
    old_factor = jnp.exp(highest - top_all)
    new_factor = jnp.exp(own_score - top_all)
    attended = (mixtures * old_factor[..., None] + own_values * new_factor[..., None]) / (
        totals * old_factor + new_factor
    )[..., None]
    attended = attended.reshape(batch_rows, heads_here * head_size).astype(jnp.bfloat16)
    branch = jnp.dot(attended, w_out, preferred_element_type=jnp.float32)
    branch_part = lax.psum_scatter(branch, "tp", scatter_dimension=1, tiled=True)
    middle = (tokens.astype(jnp.float32) + branch_part).astype(jnp.bfloat16)
    wide_mid = lax.optimization_barrier(middle).astype(jnp.float32)
    whole_mid, whole_gain = (
        lax.all_gather(middle, ("kv", "tp"), axis=1, tiled=True),
        lax.all_gather(gain_second, ("kv", "tp"), axis=0, tiled=True),
    )
    wide_whole = whole_mid.astype(jnp.float32)
    mid_mean, mid_scale = row_scales(
        jnp.sum(wide_whole, axis=1, keepdims=True),
        jnp.sum(wide_whole * wide_whole, axis=1, keepdims=True),
        wide_whole.shape[1],
    )
    normed = ((wide_whole - mid_mean) * mid_scale * whole_gain.astype(jnp.float32)).astype(
        jnp.bfloat16
    )
    gate_acc = jnp.dot(normed, w_gate, preferred_element_type=jnp.float32)
    up_acc = jnp.dot(normed, w_up, preferred_element_type=jnp.float32)
    hidden = (jax.nn.silu(gate_acc) * up_acc).astype(jnp.bfloat16)
    channel = lax.psum_scatter(
        jnp.dot(hidden, w_down, preferred_element_type=jnp.float32),
        ("kv", "tp"),
        scatter_dimension=1,
        tiled=True,
    )
    layer_out = (wide_mid + channel).astype(jnp.bfloat16)
    return (layer_out, new_keys, new_values, new_forget)


def solution(mesh):
    in_specs = (
        P(None, ("kv", "tp")),
        P(("kv", "tp")),
        P("kv", "tp"),
        P("kv", "tp"),
        P("kv", "tp"),
        P("kv", None),
        P("tp"),
        P(None, "kv", "tp"),
        P(None, "kv", "tp"),
        P(None, "tp", "kv"),
        P("tp", "kv"),
        P(("kv", "tp")),
        P(None, ("kv", "tp")),
        P(None, ("kv", "tp")),
        P(("kv", "tp"), None),
    )
    out_specs = (P(None, ("kv", "tp")), P(None, "tp"), P(None, "tp"), P(None, "tp"))
    return jax.shard_map(local, mesh=mesh, in_specs=in_specs, out_specs=out_specs, check_vma=False)
```

profile of v0, /device:TPU:0, one launch (start us, length us, event | category | flops | bytes accessed | tf_op | source)
XLA Modules:
  0.0 462.0 jit_solution(16815354026770235516)
XLA Ops:
  7.2 6.3 %all-gather.4 = bf16[4,1,128]{2,1,0:T(2,128)(2,1)S(1)} all-gather(bf16[1,1,128]{2,1,0:T(2,128)(2,1)} %bitcast.103), channel_id=1, replica_groups=mesh['kv'=8,'tp'=4] {'tp'}, dimensions={0}, use_global_device_ids=true | all-gather | bytes 1280 | tf_op jit(solution)/shard_map/all_gather | solution.py:71
  13.6 5.6 %all_gather.36 = bf16[4,512]{1,0:T(4,128)(2,1)S(1)} all-gather(bf16[4,128]{1,0:T(4,128)(2,1)} %param.19), channel_id=1, replica_groups=mesh['kv'=8,'tp'=4] {'tp'}, dimensions={1}, use_global_device_ids=true | all-gather | bytes 5120 | tf_op jit(solution)/shard_map/all_gather | solution.py:70
  20.9 1.2 fusion.39
  22.1 1.2 fusion.29
  23.3 1.2 fusion.37
  24.6 1.2 fusion.27
  25.8 1.2 fusion.42
  27.0 1.2 fusion.32
  28.2 38.0 %all-reduce = (f32[4,512]{1,0:T(4,128)S(1)}, f32[512]{0:T(512)S(1)}, f32[4]{0:T(128)S(1)}, f32[4]{0:T(128)S(1)}, f32[4,512]{1,0:T(4,128)S(1)}, /*index=5*/f32[51...) all-reduce(f32[4,512]{1,0:T(4,128)S(1)} %fusion.37, ...), channel_id=1, replica_groups=mesh['kv'=8,'tp'=4] {'kv'}, use_global_device_ids=true, to_apply=%region_18.19 | all-reduce | flops 7728 | bytes 61824 | tf_op jit(solution)/shard_map/psum | solution.py:80
  67.7 11.6 %copy.25 = bf16[4,2048,512]{1,2,0:T(8,128)(2,1)} copy(bf16[4,2048,512]{2,1,0:T(8,128)(2,1)} %param.26) | data formatting | bytes 16777216 | tf_op args[7]
  79.3 9.1 %reduce-window.6 = f32[4,8,16,128]{3,2,1,0:T(8,128)S(1)} reduce-window(f32[4,8,16,128]{3,2,1,0:T(8,128)S(1)} %copy.26, f32[]{:T(128)} %constant.91.clone.1), window={size=1x1x1x128 pad=0_0x0_0x0_0x127_0}, to_apply=%region_8.0 | reduce-window | flops 8323072 | bytes 524292 | tf_op jit(solution)/shard_map/reduce-window
  89.8 26.1 %all-gather = f32[32,8,1]{1,2,0:T(1,128)S(1)} all-gather(f32[4,8,1]{1,2,0:T(1,128)S(1)} %copy.41), channel_id=2, replica_groups=mesh['kv'=8,'tp'=4] {'kv'}, dimensions={0}, use_global_device_ids=true | all-gather | bytes 1152 | tf_op jit(solution)/shard_map/all_gather | solution.py:13
  116.1 11.4 %copy.28 = bf16[4,2048,512]{1,2,0:T(8,128)(2,1)} copy(bf16[4,2048,512]{2,1,0:T(8,128)(2,1)} %param.27) | data formatting | bytes 16777216 | tf_op args[8]
  127.6 4.7 %fusion.54 = f32[4,8,1,2048]{3,2,1,0:T(1,128)S(1)} fusion(bf16[4,8,64,1]{2,3,1,0:T(2,128)(2,1)S(1)} %reshape.143, bf16[4,2048,8,64]{1,3,2,0:T(8,128)(2,1)} %bitcast.86), kind=kOutput, calls=%fused_computation.82 | convolution fusion | flops 8388608 | bytes 8654848 | tf_op jit(solution)/shard_map/bhd,bshd->bhs/dot_general | solution.py:118
  133.4 2.3 fusion.5
  135.6 30.5 %all-gather.3 = f32[32,8,64]{2,1,0:T(8,128)S(1)} all-gather(f32[4,8,64]{2,1,0:T(8,128)S(1)} %all_gather.48), channel_id=5, replica_groups=mesh['kv'=8,'tp'=4] {'kv'}, dimensions={0}, use_global_device_ids=true | all-gather | bytes 73728 | tf_op jit(solution)/shard_map/all_gather | solution.py:24
  166.2 26.1 %all-gather.6 = f32[8,4,8]{2,1,0:T(4,128)S(1)} all-gather(f32[1,4,8]{2,1,0:T(4,128)S(1)} %bitcast.102), channel_id=4, replica_groups=mesh['kv'=8,'tp'=4] {'kv'}, dimensions={0}, use_global_device_ids=true | all-gather | bytes 1152 | tf_op jit(solution)/shard_map/all_gather | solution.py:24
  192.8 26.1 %all-gather.5 = f32[8,4,8]{2,1,0:T(4,128)S(1)} all-gather(f32[1,4,8]{2,1,0:T(4,128)S(1)} %bitcast.96), channel_id=3, replica_groups=mesh['kv'=8,'tp'=4] {'kv'}, dimensions={0}, use_global_device_ids=true | all-gather | bytes 1152 | tf_op jit(solution)/shard_map/all_gather | solution.py:24
  219.6 9.4 %while.32 = (s32[]{:T(128)}, f32[4,8]{1,0:T(4,128)}, f32[4,8]{1,0:T(4,128)}, f32[4,8,64]{2,1,0:T(8,128)S(1)}, f32[8,4,8]{2,1,0:T(4,128)}, /*index=5*/f32[8,4,8]{...) while((s32[]{:T(128)}, f32[4,8]{1,0:T(4,128)}, f32[4,8]{1,0:T(4,128)}, ...), condition=%wide.region_15.16_spmd, body=%wide.region_14.15_spmd.sunk | while | flops 6341 | bytes 26007 | solution.py:30
  219.6 1.3 fusion.71
  220.9 1.3 fusion.71
  222.2 1.3 fusion.71
  223.6 1.3 fusion.71
  224.9 1.3 fusion.71
  226.3 1.3 fusion.71
  227.6 1.3 fusion.71
  232.2 1.0 convolution_bitcast_fusion.1
  233.3 38.0 %all-gather.7 = bf16[32,1,128]{2,1,0:T(2,128)(2,1)S(1)} all-gather(bf16[1,1,128]{2,1,0:T(2,128)(2,1)} %bitcast.104), channel_id=1, replica_groups=mesh['kv'=8,'tp'=4] {'kv','tp'}, dimensions={0}, use_global_device_ids=true | all-gather | bytes 8448 | tf_op jit(solution)/shard_map/all_gather | solution.py:156
  272.9 36.9 %all_gather.46 = bf16[4,4096]{1,0:T(4,128)(2,1)S(1)} all-gather(bf16[4,128]{1,0:T(4,128)(2,1)S(1)} %add_convert_fusion.1), channel_id=1, replica_groups=mesh['kv'=8,'tp'=4] {'kv','tp'}, dimensions={1}, use_global_device_ids=true | all-gather | bytes 33792 | tf_op jit(solution)/shard_map/all_gather | solution.py:155
  310.0 2.7 fusion.46
  312.6 5.5 %convolution_bitcast_fusion = f32[4096,4]{1,0:T(8,128)} fusion(bf16[352,4096]{1,0:T(8,128)(2,1)S(1)} %copy-done, bf16[4096,352]{0,1:T(8,128)(2,1)} %param.32, f32[4,352]{1,0:T(4,128)S(1)} %fusion.46, bf16[4,4096]{1,0:T(4,128)(2,1)S(1)} %all_gather.46, f32[4096]{0:T(1024)S(1)} %bitcast.91, f32[4]{0:T(128)S(1)} %get-tuple-element.295, f32[4]{0:T(128)S(1)} %get-tuple-element.294), kind=kOutput, calls=%fused_computation.9 | convolution fusion | flops 23159040 | bytes 5887520
  318.2 135.5 %reduce-scatter.9.cloned.1.call-done = f32[128,4]{1,0:T(8,128)} async-done(((f32[4096,4]{1,0:T(8,128)}), f32[128,4]{1,0:T(8,128)}) %reduce-scatter.9.cloned.1.call-update) | async-done | bytes 2064
  (72 shorter events, 14.4 us)
Async XLA Ops:
  7.2 305.5 %copy-start = (bf16[352,4096]{1,0:T(8,128)(2,1)S(1)}, bf16[352,4096]{1,0:T(8,128)(2,1)}, u32[]{:S(2)}) copy-start(bf16[352,4096]{1,0:T(8,128)(2,1)} %param.33) | copy-start | bytes 8650756
  7.2 264.1 %reduce-scatter.7.cloned.1.call-start = ((), (), s32[]{:S(2)}) async-start(), calls=%async_computation.2 | async-start | bytes 327680
  67.7 11.6 %copy-start.3 = (f32[4,8,2048]{2,1,0:T(8,128)S(1)}, f32[4,8,2048]{2,1,0:T(8,128)}, u32[]{:S(2)}) copy-start(f32[4,8,2048]{2,1,0:T(8,128)} %param.28) | copy-start | bytes 786436
  127.5 4.7 %copy-start.6 = (f32[8]{0:T(128)S(1)}, f32[8]{0:T(128)}, u32[]{:S(2)}) copy-start(f32[8]{0:T(128)} %param.25) | copy-start | bytes 100
  127.6 5.8 %copy-start.1 = (bf16[4,2048,512]{1,2,0:T(8,128)(2,1)S(1)}, bf16[4,2048,512]{1,2,0:T(8,128)(2,1)}, u32[]{:S(2)}) copy-start(bf16[4,2048,512]{1,2,0:T(8,128)(2,1)} %copy.28) | copy-start | bytes 25165828
  133.4 98.8 %copy-start.2 = (bf16[512,512]{1,0:T(8,128)(2,1)S(1)}, bf16[512,512]{1,0:T(8,128)(2,1)}, u32[]{:S(2)}) copy-start(bf16[512,512]{1,0:T(8,128)(2,1)} %param.29) | copy-start | bytes 1572868
  192.3 27.3 %copy-start.4 = (f32[8,4,8]{2,1,0:T(4,128)}, f32[8,4,8]{2,1,0:T(4,128)S(1)}, u32[]{:S(2)}) copy-start(f32[8,4,8]{2,1,0:T(4,128)S(1)} %all-gather.6) | copy-start | bytes 3076
  218.9 0.6 copy-start.5
  233.2 220.5 %reduce-scatter.9.cloned.1.call-start = ((), (), s32[]{:S(2)}) async-start(), calls=%async_computation.3 | async-start | bytes 2162688
Sparse Core Ops, SparseCore 0:
  233.4 17.2 reduce-scatter.6
  318.3 135.3 reduce-scatter.8
where the time goes:
time: 464 us; the launch traced here: 462 us
  blocking collectives  234 us (50%)
  waiting for transfers between devices  136 us (29%)
  local copies, waits for them, and re-layouts  28.9 us (6%)
  matrix products  25.2 us (5%)
  other arithmetic  24.4 us (5%)
  between operations  14.1 us (3%)
    unnamed x4, waiting for transfers between devices  136 us
    all_gather x3, blocking collectives, merged(): everything = jax.tree.map(lambda part: lax.all_gather(part, axis), array)  82.7 us
    psum x1, blocking collectives, local(): lax.psum((jnp.dot(scaled, w_query, preferred_element_type=jnp.float32), j...  38 us
    all_gather x1, blocking collectives, local(): lax.all_gather(gain_second, ('kv', 'tp'), axis=0, tiled=True)  38 us
    all_gather x1, blocking collectives, local(): lax.all_gather(middle, ('kv', 'tp'), axis=1, tiled=True)  36.9 us
    all_gather x1, blocking collectives, prefix(): gathered = lax.all_gather(part, axis)  26.1 us
    unnamed x19, local copies, waits for them, and re-layouts  24.9 us
    another operation x3, other arithmetic  9.91 us
  transfers between devices with their start and end apart: 2, of which 1 were waited for; matrix products, arithmetic and copies ran while one was open for 0% of the time, Pallas kernels for 0%

commit v1 on v0

v1 whole, which is shorter than its diff:
```python
import functools

import jax
import jax.numpy as jnp
from jax import lax
from jax.experimental import pallas as pl
from jax.experimental.pallas import tpu as pltpu
from jax.sharding import PartitionSpec as P

epsilon = 1e-05
MESH = pl.DeviceIdType.MESH
HIGHEST = lax.Precision.HIGHEST
LANES = 128
F32 = jnp.float32
BF16 = jnp.bfloat16


def iota(shape, dim):
    return lax.broadcasted_iota(jnp.int32, shape, dim)


def row_scales(first_sum, second_sum, row_width):
    row_mean = first_sum / row_width
    spread = jnp.maximum(second_sum / row_width - row_mean * row_mean, 0.0) + epsilon
    return (row_mean, lax.rsqrt(spread))


def kernel(
    nkv,
    ntp,
    tokens_h,
    gain1_h,
    wq_h,
    wk_h,
    wv_h,
    wf_h,
    fb_h,
    pk_h,
    pv_h,
    pf_h,
    wo_h,
    gain2_h,
    wg_h,
    wu_h,
    wd_h,
    out_ref,
    nk_ref,
    nv_ref,
    nf_ref,
    tokens_v,
    gain1_v,
    gain2_v,
    wq_v,
    wk_v,
    wv_v,
    wf_v,
    fb_v,
    pk_v,
    pv_v,
    pf_v,
    wo_v,
    wg_v,
    wu_v,
    wd_v,
    gat,
    xbuf,
    qmsg,
    kvmsg,
    sfx,
    mixbuf,
    amix,
    astat,
    coef,
    bmsg,
    mpieces,
    mmsg,
    mbuf,
    gbuf,
    fsend,
    frecv,
    in_sem,
    s1,
    r1,
    sq,
    rq,
    sk,
    rk,
    sa,
    ra,
    st,
    rt,
    sb,
    rb,
    sm,
    rm,
    sf,
    rf,
):
    i = lax.axis_index("kv")
    j = lax.axis_index("tp")
    B, c0 = tokens_v.shape
    R, C = wq_v.shape
    H = wf_v.shape[1]
    h = fb_v.shape[1]
    hd = C // h
    S = pk_v.shape[1]
    D, F = wg_v.shape
    N = nkv * ntp
    scale = hd ** (-0.5)
    nc, nr = C // LANES, R // LANES

    plan = [
        (tokens_h, tokens_v),
        (gain1_h, gain1_v),
        (gain2_h, gain2_v),
        (wq_h, wq_v),
        (wf_h, wf_v),
        (wk_h, wk_v),
        (wv_h, wv_v),
        (pf_h, pf_v),
    ]
    plan += [(pk_h.at[b], pk_v.at[b]) for b in range(B)]
    plan += [(pv_h.at[b], pv_v.at[b]) for b in range(B)]
    plan += [(fb_h, fb_v), (wo_h, wo_v), (wg_h, wg_v), (wu_h, wu_v), (wd_h, wd_v)]
    loads = [
        pltpu.make_async_copy(src, dst, in_sem.at[n]) for n, (src, dst) in enumerate(plan)
    ]
    for load in loads:
        load.start()
    l_tok, l_g1, l_g2, l_wq, l_wf, l_wk, l_wv, l_pf = loads[:8]
    l_pk, l_pv = loads[8 : 8 + B], loads[8 + B : 8 + 2 * B]
    l_fb, l_wo, l_wg, l_wu, l_wd = loads[8 + 2 * B :]

    barrier = pltpu.get_barrier_semaphore()
    for a in range(nkv):
        for b in range(ntp):
            if a or b:
                pl.semaphore_signal(
                    barrier,
                    inc=1,
                    device_id=(lax.rem(i + a, nkv), lax.rem(j + b, ntp)),
                    device_id_type=MESH,
                )

    pending = []

    def to_kv(buf, ssem, rsem):
        for o in range(1, nkv):
            copy = pltpu.make_async_remote_copy(
                src_ref=buf.at[i],
                dst_ref=buf.at[i],
                send_sem=ssem.at[o],
                recv_sem=rsem.at[o],
                device_id=(lax.rem(i + o, nkv), j),
                device_id_type=MESH,
            )
            copy.start()
            pending.append(copy)

    def from_kv(buf, ssem, rsem):
        for o in range(1, nkv):
            slot = lax.rem(i + nkv - o, nkv)
            pltpu.make_async_remote_copy(
                src_ref=buf.at[slot],
                dst_ref=buf.at[slot],
                send_sem=ssem.at[o],
                recv_sem=rsem.at[o],
                device_id=(slot, j),
                device_id_type=MESH,
            ).wait_recv()

    def to_tp(buf, ssem, rsem):
        for o in range(1, ntp):
            copy = pltpu.make_async_remote_copy(
                src_ref=buf.at[j],
                dst_ref=buf.at[j],
                send_sem=ssem.at[o],
                recv_sem=rsem.at[o],
                device_id=(i, lax.rem(j + o, ntp)),
                device_id_type=MESH,
            )
            copy.start()
            pending.append(copy)

    def from_tp(buf, ssem, rsem):
        for o in range(1, ntp):
            slot = lax.rem(j + ntp - o, ntp)
            pltpu.make_async_remote_copy(
                src_ref=buf.at[slot],
                dst_ref=buf.at[slot],
                send_sem=ssem.at[o],
                recv_sem=rsem.at[o],
                device_id=(i, slot),
                device_id_type=MESH,
            ).wait_recv()

    l_tok.wait()
    l_g1.wait()
    l_g2.wait()
    gat[j, 0:B, :] = tokens_v[...].astype(F32)
    gat[j, B : B + 1, :] = gain1_v[...].astype(F32)
    gat[j, B + 1 : B + 2, :] = gain2_v[...].astype(F32)
    gat[j, B + 2 : 8, :] = jnp.zeros((6 - B, c0), F32)
    pl.semaphore_wait(barrier, N - 1)
    to_tp(gat, s1, r1)
    l_wq.wait()
    l_wf.wait()
    from_tp(gat, s1, r1)
    for t in range(ntp):
        xbuf[:, t * c0 : (t + 1) * c0] = gat[t]

    every = xbuf[...]
    rows = every[0:B]
    gain_b = jnp.broadcast_to(every[B : B + 1], every.shape)
    row_id = iota(every.shape, 0)
    lhs = jnp.where(row_id < B, every * gain_b, jnp.where(row_id == B, gain_b, 0.0)).astype(BF16)

    def product(weight):
        return jnp.dot(lhs, weight[...], preferred_element_type=F32)

    def spread(buf, at, row, count):
        if count < B:
            buf[i, :, at : at + LANES] = jnp.zeros((B, LANES), F32)
        for r in range(count):
            buf[i, r : r + 1, at : at + LANES] = row[:, r * LANES : (r + 1) * LANES]

    part = product(wq_v)
    qmsg[i, :, 0:C] = part[0:B]
    spread(qmsg, C, part[B : B + 1], nc)
    part = product(wf_v)
    aux = C + LANES
    qmsg[i, :, aux : aux + LANES] = jnp.zeros((B, LANES), F32)
    qmsg[i, :, aux : aux + H] = part[0:B]
    qmsg[i, :, aux + H : aux + 2 * H] = jnp.broadcast_to(part[B : B + 1], (B, H))
    qmsg[i, :, aux + 2 * H : aux + 2 * H + 1] = jnp.sum(rows, axis=1, keepdims=True)
    qmsg[i, :, aux + 2 * H + 1 : aux + 2 * H + 2] = jnp.sum(rows * rows, axis=1, keepdims=True)
    to_kv(qmsg, sq, rq)

    l_wk.wait()
    part = product(wk_v)
    kvmsg[i, :, 0:C] = part[0:B]
    spread(kvmsg, 2 * C, part[B : B + 1], nc)
    l_wv.wait()
    part = product(wv_v)
    kvmsg[i, :, C : 2 * C] = part[0:B]
    spread(kvmsg, 2 * C + LANES, part[B : B + 1], nc)
    spread(kvmsg, 2 * C + 2 * LANES, every[B + 1 : B + 2], nr)
    to_kv(kvmsg, sk, rk)

    l_pf.wait()
    later = (iota((LANES, LANES), 0) > iota((LANES, LANES), 1)).astype(F32)
    carry = jnp.zeros((B * h, 1), F32)
    for c in reversed(range(S // LANES)):
        cols = slice(c * LANES, (c + 1) * LANES)
        chunk = jnp.concatenate([pf_v[b, :, cols] for b in range(B)], axis=0)
        inside = jnp.dot(chunk, later, precision=HIGHEST, preferred_element_type=F32)
        whole = inside + carry
        for b in range(B):
            sfx[b, :, cols] = whole[b * h : (b + 1) * h]
        carry = carry + (inside[:, 0:1] + chunk[:, 0:1])

    from_kv(qmsg, sq, rq)
    total = qmsg[0]
    for n in range(1, nkv):
        total = total + qmsg[n]
    moments = total[:, aux + 2 * H : aux + 2 * H + 2]
    mean, factor = row_scales(moments[:, 0:1], moments[:, 1:2], D)

    def whole_row(array, at, count):
        return jnp.concatenate([array[r : r + 1, at : at + LANES] for r in range(count)], axis=1)

    def finish(product_, gain_row):
        return factor * (product_ - mean * gain_row)

    query = finish(total[:, 0:C], whole_row(total, C, nc)).astype(BF16).astype(F32)

    head_of = iota((h, C), 1) // hd
    mine = head_of == iota((h, C), 0)
    head_row = iota((h, LANES), 0)
    lane = iota((h, LANES), 1)
    for b in range(B):
        spread_q = jnp.where(mine, jnp.broadcast_to(query[b : b + 1], (h, C)), 0.0).astype(BF16)
        l_pk[b].wait()
        scores = lax.dot_general(
            spread_q, pk_v[b], (((1,), (1,)), ((), ())), preferred_element_type=F32
        )
        logits = scores * scale + sfx[b]
        top = jnp.max(logits, axis=1, keepdims=True)
        weights = jnp.exp(logits - top)
        amount = jnp.sum(weights, axis=1, keepdims=True)
        l_pv[b].wait()
        mixed = jnp.dot(weights.astype(BF16), pv_v[b], preferred_element_type=F32)
        mixbuf[b : b + 1, :] = jnp.sum(jnp.where(mine, mixed, 0.0), axis=0, keepdims=True)
        marks = (
            jnp.where(lane == head_row, top, 0.0)
            + jnp.where(lane == head_row + 32, amount, 0.0)
            + jnp.where(lane == head_row + 64, carry[b * h : (b + 1) * h], 0.0)
        )
        astat[i, b : b + 1, :] = jnp.sum(marks, axis=0, keepdims=True)
    amix[i] = mixbuf[...].astype(BF16)
    to_kv(astat, st, rt)
    to_kv(amix, sa, ra)

    from_kv(kvmsg, sk, rk)
    pair = kvmsg[0, :, 0 : 2 * C + 2 * LANES]
    for n in range(1, nkv):
        pair = pair + kvmsg[n, :, 0 : 2 * C + 2 * LANES]
    for n in range(nkv):
        for r in range(nr):
            at = n * R + r * LANES
            gbuf[0:1, at : at + LANES] = kvmsg[n, r : r + 1, 2 * C + 2 * LANES : 2 * C + 3 * LANES]
    new_keys = finish(pair[:, 0:C], whole_row(pair, 2 * C, nc)).astype(BF16)
    new_values = finish(pair[:, C : 2 * C], whole_row(pair, 2 * C + LANES, nc)).astype(BF16)
    nk_ref[...] = new_keys
    nv_ref[...] = new_values
    pre = finish(total[:, aux : aux + H], total[:, aux + H : aux + 2 * H])
    pick = (iota((H, LANES), 0) == iota((H, LANES), 1) + j * h).astype(F32)
    l_fb.wait()
    gates = jnp.dot(pre, pick, precision=HIGHEST, preferred_element_type=F32)[:, 0:h] + fb_v[...]
    new_forget = jnp.minimum(gates, 0.0) - jnp.log1p(jnp.exp(-jnp.abs(gates)))
    nf_ref[...] = new_forget
    expand = (iota((LANES, C), 0) == iota((LANES, C), 1) // hd).astype(F32)
    gather = (iota((C, LANES), 0) // hd == iota((C, LANES), 1)).astype(F32)
    own = (
        jnp.dot(
            query * new_keys.astype(F32), gather, precision=HIGHEST, preferred_element_type=F32
        )[:, 0:h]
        * scale
    )
    coef[...] = jnp.zeros(coef.shape, F32)
    l_wo.wait()

    from_kv(astat, st, rt)
    tops, amounts = [None] * nkv, [None] * nkv
    behind = new_forget
    peak = own
    for n in reversed(range(nkv)):
        tops[n] = astat[n, :, 0:h] + behind
        amounts[n] = astat[n, :, 32 : 32 + h]
        behind = behind + astat[n, :, 64 : 64 + h]
        peak = jnp.maximum(peak, tops[n])
    own_part = jnp.exp(own - peak)
    bottom = own_part
    parts = []
    for n in range(nkv):
        parts.append(jnp.exp(tops[n] - peak))
        bottom = bottom + amounts[n] * parts[n]
    for n, one in enumerate(parts + [own_part]):
        coef[n * B : (n + 1) * B, 0:h] = one / bottom
    wide = jnp.dot(coef[...], expand, precision=HIGHEST, preferred_element_type=F32)
    attended = wide[nkv * B : (nkv + 1) * B] * new_values.astype(F32)
    from_kv(amix, sa, ra)
    for n in range(nkv):
        attended = attended + wide[n * B : (n + 1) * B] * amix[n].astype(F32)

    bmsg[j] = jnp.dot(attended.astype(BF16), wo_v[...], preferred_element_type=F32)
    to_tp(bmsg, sb, rb)
    from_tp(bmsg, sb, rb)
    branch = bmsg[0]
    for t in range(1, ntp):
        branch = branch + bmsg[t]
    middle = (rows + branch).astype(BF16)
    mmsg[i] = middle
    to_kv(mmsg, sm, rm)
    for t in range(ntp):
        mpieces[t] = middle[:, t * c0 : (t + 1) * c0].astype(F32)
    l_wg.wait()
    l_wu.wait()
    l_wd.wait()
    from_kv(mmsg, sm, rm)
    for n in range(nkv):
        mbuf[:, n * R : (n + 1) * R] = mmsg[n].astype(F32)
    wide_mid = mbuf[...]
    mid_mean, mid_scale = row_scales(
        jnp.sum(wide_mid, axis=1, keepdims=True),
        jnp.sum(wide_mid * wide_mid, axis=1, keepdims=True),
        D,
    )
    normed = ((wide_mid - mid_mean) * mid_scale * gbuf[...]).astype(BF16)
    gate = jnp.dot(normed, wg_v[...], preferred_element_type=F32)
    up = jnp.dot(normed, wu_v[...], preferred_element_type=F32)
    hidden = (gate / (1.0 + jnp.exp(-gate)) * up).astype(BF16)
    down = jnp.dot(hidden, wd_v[...], preferred_element_type=F32)
    for p in range(N):
        fsend[p] = down[:, p * c0 : (p + 1) * c0]
    me = i * ntp + j
    for a in reversed(range(nkv)):
        for b in range(ntp):
            if a or b:
                there = (lax.rem(i + a, nkv), lax.rem(j + b, ntp))
                copy = pltpu.make_async_remote_copy(
                    src_ref=fsend.at[there[0] * ntp + there[1]],
                    dst_ref=frecv.at[me],
                    send_sem=sf.at[a * ntp + b],
                    recv_sem=rf.at[a * ntp + b],
                    device_id=there,
                    device_id_type=MESH,
                )
                copy.start()
                pending.append(copy)
    frecv[me] = fsend[me]
    for a in range(nkv):
        for b in range(ntp):
            if a or b:
                there = (lax.rem(i + nkv - a, nkv), lax.rem(j + ntp - b, ntp))
                slot = there[0] * ntp + there[1]
                pltpu.make_async_remote_copy(
                    src_ref=fsend.at[slot],
                    dst_ref=frecv.at[slot],
                    send_sem=sf.at[a * ntp + b],
                    recv_sem=rf.at[a * ntp + b],
                    device_id=there,
                    device_id_type=MESH,
                ).wait_recv()
    channel = frecv[0]
    for p in range(1, N):
        channel = channel + frecv[p]
    out_ref[...] = (mpieces[j] + channel).astype(BF16)
    for copy in pending:
        copy.wait_send()


def local(nkv, ntp, *arrays):
    (tokens, gain1, wq, wk, wv, wf, fb, pk, pv, pf, wo, gain2, wg, wu, wd) = arrays
    gain1, gain2, fb = gain1[None, :], gain2[None, :], fb[None, :]
    arrays = (tokens, gain1, wq, wk, wv, wf, fb, pk, pv, pf, wo, gain2, wg, wu, wd)
    B, c0 = tokens.shape
    R, C = wq.shape
    h = fb.shape[1]
    D, F = wg.shape
    S = pk.shape[1]
    N = nkv * ntp
    dma = lambda n: pltpu.SemaphoreType.DMA((n,))
    scratch = [
        pltpu.VMEM(a.shape, a.dtype)
        for a in (tokens, gain1, gain2, wq, wk, wv, wf, fb, pk, pv, pf, wo, wg, wu, wd)
    ]
    scratch += [
        pltpu.VMEM((ntp, 8, c0), F32),
        pltpu.VMEM((8, R), F32),
        pltpu.VMEM((nkv, B, C + 2 * LANES), F32),
        pltpu.VMEM((nkv, B, 2 * C + 3 * LANES), F32),
        pltpu.VMEM((B, h, S), F32),
        pltpu.VMEM((B, C), F32),
        pltpu.VMEM((nkv, B, C), BF16),
        pltpu.VMEM((nkv, B, LANES), F32),
        pltpu.VMEM(((nkv + 1) * B, LANES), F32),
        pltpu.VMEM((ntp, B, R), F32),
        pltpu.VMEM((ntp, B, c0), F32),
        pltpu.VMEM((nkv, B, R), BF16),
        pltpu.VMEM((B, D), F32),
        pltpu.VMEM((1, D), F32),
        pltpu.VMEM((N, B, c0), F32),
        pltpu.VMEM((N, B, c0), F32),
        dma(13 + 2 * B),
    ]
    for n in (ntp, nkv, nkv, nkv, nkv, ntp, nkv, N):
        scratch += [dma(n), dma(n)]
    vmem = pl.BlockSpec(memory_space=pltpu.VMEM)
    return pl.pallas_call(
        functools.partial(kernel, nkv, ntp),
        out_shape=(
            jax.ShapeDtypeStruct((B, c0), BF16),
            jax.ShapeDtypeStruct((B, C), BF16),
            jax.ShapeDtypeStruct((B, C), BF16),
            jax.ShapeDtypeStruct((B, h), F32),
        ),
        in_specs=[pl.BlockSpec(memory_space=pl.ANY)] * len(arrays),
        out_specs=(vmem,) * 4,
        scratch_shapes=scratch,
        compiler_params=pltpu.CompilerParams(
            collective_id=0, has_side_effects=True, vmem_limit_bytes=60 * 2**20
        ),
    )(*arrays)


def solution(mesh):
    in_specs = (
        P(None, ("kv", "tp")),
        P(("kv", "tp")),
        P("kv", "tp"),
        P("kv", "tp"),
        P("kv", "tp"),
        P("kv", None),
        P("tp"),
        P(None, "kv", "tp"),
        P(None, "kv", "tp"),
        P(None, "tp", "kv"),
        P("tp", "kv"),
        P(("kv", "tp")),
        P(None, ("kv", "tp")),
        P(None, ("kv", "tp")),
        P(("kv", "tp"), None),
    )
    out_specs = (P(None, ("kv", "tp")), P(None, "tp"), P(None, "tp"), P(None, "tp"))
    step = functools.partial(local, mesh.shape["kv"], mesh.shape["tp"])
    return jax.shard_map(step, mesh=mesh, in_specs=in_specs, out_specs=out_specs, check_vma=False)
```

time: 464 us -> 55.3 us (0.12)
  blocking collectives: 234 us -> 0 us
  waiting for transfers between devices: 136 us -> 0 us
  Pallas kernels: 0 us -> 40.2 us
  matrix products: 25.2 us -> 0 us
  other arithmetic: 24.4 us -> 0 us
  local copies, waits for them, and re-layouts: 28.9 us -> 14.1 us
  between operations: 14.1 us -> 0.65 us
    all_gather x8 -> x0, blocking collectives: 196 us -> none  [the longest x3 82.7 us: merged(): everything = jax.tree.map(lambda part: lax.all_gather(part, axis), array)]
    unnamed x4 -> x0, waiting for transfers between devices: 136 us -> none
    pallas_call x0 -> x1, Pallas kernels: none -> 40.2 us  [local(): pl.pallas_call(functools.partial(kernel, nkv, ntp), out_shape=(jax.ShapeD...]
    psum x1 -> x0, blocking collectives: 38 us -> none  [local(): lax.psum((jnp.dot(scaled, w_query, preferred_element_type=jnp.float32), j...]
    dot_general x11 -> x0, matrix products: 18.6 us -> none  [the longest x1 4.72 us: local(): jnp.einsum('bhd,bshd->bhs', query_heads, key_heads, preferred_element_typ...]
    add x23 -> x0, other arithmetic: 10.9 us -> none  [the longest x7 8.89 us: combine_blocks(): totals = left_part[1] * left_factor + right_part[1] * right_factor]
    unnamed x19 -> x9, local copies, waits for them, and re-layouts: 24.9 us -> 14.1 us
    another operation x3 -> x0, other arithmetic: 9.91 us -> none
  transfers between devices with their start and end apart: 2 -> 0, of which waited for: 1 -> 0; matrix products, arithmetic and copies ran while one was open for 0% -> 0% of each run, Pallas kernels for 0% -> 0%
where the time goes in v1:
time: 55.3 us; the launch traced here: 55 us
  Pallas kernels  40.2 us (73%)
  local copies, waits for them, and re-layouts  14.1 us (25%)
  between operations  0.65 us (1%)
    pallas_call x1, Pallas kernels, local(): pl.pallas_call(functools.partial(kernel, nkv, ntp), out_shape=(jax.ShapeD...  40.2 us
    unnamed x9, local copies, waits for them, and re-layouts  14.1 us

profile of v1, /device:TPU:0, one launch (start us, length us, event | category | flops | bytes accessed | tf_op | source)
XLA Modules:
  0.0 55.0 jit_solution(8456681007300103790)
XLA Ops:
  0.6 0.0 copy-start
  0.6 1.7 %copy.19.wf_h = bf16[512,32]{1,0:T(8,128)(2,1)} copy(bf16[512,32]{0,1:T(8,128)(2,1)} %param.20) | data formatting | bytes 65536 | tf_op args[5]
  2.3 4.6 %copy.20.wg_h = bf16[4096,352]{1,0:T(8,128)(2,1)} copy(bf16[4096,352]{0,1:T(8,128)(2,1)} %param.27) | data formatting | bytes 5767168 | tf_op args[12]
  6.9 0.0 copy-done
  6.9 2.8 %copy.21.wu_h = bf16[4096,352]{1,0:T(8,128)(2,1)} copy(bf16[4096,352]{0,1:T(8,128)(2,1)S(1)} %copy-done) | data formatting | bytes 5767168 | tf_op args[13]
  9.7 40.2 %shard_map.174 = (bf16[4,128]{1,0:T(4,128)(2,1)}, bf16[4,512]{1,0:T(4,128)(2,1)}, bf16[4,512]{1,0:T(4,128)(2,1)}, f32[4,8]{1,0:T(4,128)}) custom-call(bf16[4,128]{1,0:T(4,128)(2,1)} %tokens_h.1, bf16[1,128]{1,0:T(2,128)(2,1)} %bitcast.3, bf16[512,512]{1,0:T(8,128)(2,1)} %wq_h.1, bf16[512,512]{1,0:T(8,128)(2,1)} %wk_h.1, bf16[512,512]{1,0:T(8,128)(2,1)} %wv_h.1, ...), custom_call_target="tpu_custom_call" | custom-call | tf_op jit(solution)/shard_map/pallas_call | solution.py:460
  49.9 1.2 %copy.26 = bf16[4,128]{1,0:T(4,128)(2,1)} copy(bf16[4,128]{1,0:T(4,128)(2,1)} %get-tuple-element.8) | data formatting | bytes 2048
  51.2 1.3 %copy.27 = bf16[4,512]{1,0:T(4,128)(2,1)} copy(bf16[4,512]{1,0:T(4,128)(2,1)} %get-tuple-element.9) | data formatting | bytes 8192
  52.4 1.3 %copy.28 = bf16[4,512]{1,0:T(4,128)(2,1)} copy(bf16[4,512]{1,0:T(4,128)(2,1)} %get-tuple-element.10) | data formatting | bytes 8192
  53.7 1.2 %copy.29 = f32[4,8]{1,0:T(4,128)} copy(f32[4,8]{1,0:T(4,128)} %get-tuple-element.11) | data formatting | bytes 256
Async XLA Ops:
  0.6 6.3 %copy-start = (bf16[4096,352]{0,1:T(8,128)(2,1)S(1)}, bf16[4096,352]{0,1:T(8,128)(2,1)}, u32[]{:S(2)}) copy-start(bf16[4096,352]{0,1:T(8,128)(2,1)} %param.28) | copy-start | bytes 8650756

commit v2 on v1

--- a/solution.py
+++ b/solution.py
@@ -17,6 +17,10 @@
 
 def iota(shape, dim):
     return lax.broadcasted_iota(jnp.int32, shape, dim)
+
+
+def across(left, right):
+    return lax.dot_general(left, right, (((1,), (1,)), ((), ())), preferred_element_type=F32)
 
 
 def row_scales(first_sum, second_sum, row_width):
@@ -100,11 +104,11 @@
     j = lax.axis_index("tp")
     B, c0 = tokens_v.shape
     R, C = wq_v.shape
-    H = wf_v.shape[1]
+    H = wf_v.shape[0]
     h = fb_v.shape[1]
     hd = C // h
     S = pk_v.shape[1]
-    D, F = wg_v.shape
+    F, D = wg_v.shape
     N = nkv * ntp
     scale = hd ** (-0.5)
     nc, nr = C // LANES, R // LANES
@@ -227,7 +231,7 @@
     part = product(wq_v)
     qmsg[i, :, 0:C] = part[0:B]
     spread(qmsg, C, part[B : B + 1], nc)
-    part = product(wf_v)
+    part = across(lhs, wf_v[...])
     aux = C + LANES
     qmsg[i, :, aux : aux + LANES] = jnp.zeros((B, LANES), F32)
     qmsg[i, :, aux : aux + H] = part[0:B]
@@ -281,10 +285,7 @@
     for b in range(B):
         spread_q = jnp.where(mine, jnp.broadcast_to(query[b : b + 1], (h, C)), 0.0).astype(BF16)
         l_pk[b].wait()
-        scores = lax.dot_general(
-            spread_q, pk_v[b], (((1,), (1,)), ((), ())), preferred_element_type=F32
-        )
-        logits = scores * scale + sfx[b]
+        logits = across(spread_q, pk_v[b]) * scale + sfx[b]
         top = jnp.max(logits, axis=1, keepdims=True)
         weights = jnp.exp(logits - top)
         amount = jnp.sum(weights, axis=1, keepdims=True)
@@ -377,8 +378,8 @@
         D,
     )
     normed = ((wide_mid - mid_mean) * mid_scale * gbuf[...]).astype(BF16)
-    gate = jnp.dot(normed, wg_v[...], preferred_element_type=F32)
-    up = jnp.dot(normed, wu_v[...], preferred_element_type=F32)
+    gate = across(normed, wg_v[...])
+    up = across(normed, wu_v[...])
     hidden = (gate / (1.0 + jnp.exp(-gate)) * up).astype(BF16)
     down = jnp.dot(hidden, wd_v[...], preferred_element_type=F32)
     for p in range(N):
@@ -420,14 +421,26 @@
         copy.wait_send()
 
 
+def hand_over(*refs):
+    count = len(refs) // 3
+    copies = [
+        pltpu.make_async_copy(refs[n], refs[count + n], refs[2 * count + n]) for n in range(count)
+    ]
+    for copy in copies:
+        copy.start()
+    for copy in copies:
+        copy.wait()
+
+
 def local(nkv, ntp, *arrays):
     (tokens, gain1, wq, wk, wv, wf, fb, pk, pv, pf, wo, gain2, wg, wu, wd) = arrays
     gain1, gain2, fb = gain1[None, :], gain2[None, :], fb[None, :]
+    wf, wg, wu = wf.T, wg.T, wu.T
     arrays = (tokens, gain1, wq, wk, wv, wf, fb, pk, pv, pf, wo, gain2, wg, wu, wd)
     B, c0 = tokens.shape
     R, C = wq.shape
     h = fb.shape[1]
-    D, F = wg.shape
+    F, D = wg.shape
     S = pk.shape[1]
     N = nkv * ntp
     dma = lambda n: pltpu.SemaphoreType.DMA((n,))
@@ -457,7 +470,7 @@
     for n in (ntp, nkv, nkv, nkv, nkv, ntp, nkv, N):
         scratch += [dma(n), dma(n)]
     vmem = pl.BlockSpec(memory_space=pltpu.VMEM)
-    return pl.pallas_call(
+    results = pl.pallas_call(
         functools.partial(kernel, nkv, ntp),
         out_shape=(
             jax.ShapeDtypeStruct((B, c0), BF16),
@@ -472,6 +485,13 @@
             collective_id=0, has_side_effects=True, vmem_limit_bytes=60 * 2**20
         ),
     )(*arrays)
+    return pl.pallas_call(
+        hand_over,
+        out_shape=tuple(jax.ShapeDtypeStruct(one.shape, one.dtype) for one in results),
+        in_specs=[vmem] * 4,
+        out_specs=(pl.BlockSpec(memory_space=pl.ANY),) * 4,
+        scratch_shapes=[pltpu.SemaphoreType.DMA] * 4,
+    )(*results)
 
 
 def solution(mesh):

time: 55.3 us -> 43.1 us (0.78)
  local copies, waits for them, and re-layouts: 14.1 us -> 0 us
  Pallas kernels: 40.2 us -> 42.2 us
    unnamed x9 -> x0, local copies, waits for them, and re-layouts: 14.1 us -> none
    pallas_call x0 -> x1, Pallas kernels: none -> 1.34 us  [local(): pl.pallas_call(hand_over, out_shape=tuple((jax.ShapeDtypeStruct(one.shape...]
    pallas_call x1, Pallas kernels: 40.2 us -> 40.9 us  [local(): pl.pallas_call(functools.partial(kernel, nkv, ntp), out_shape=(jax.ShapeD...]
where the time goes in v2:
time: 43.1 us; the launch traced here: 42.9 us
  Pallas kernels  42.2 us (98%)
  between operations  0.65 us (2%)
    pallas_call x1, Pallas kernels, local(): pl.pallas_call(functools.partial(kernel, nkv, ntp), out_shape=(jax.ShapeD...  40.9 us
    pallas_call x1, Pallas kernels, local(): pl.pallas_call(hand_over, out_shape=tuple((jax.ShapeDtypeStruct(one.shape...  1.34 us

profile of v2, /device:TPU:0, one launch (start us, length us, event | category | flops | bytes accessed | tf_op | source)
XLA Modules:
  0.0 42.9 jit_solution(11726794273237693516)
XLA Ops:
  0.6 40.9 %shard_map.174 = (bf16[4,128]{1,0:T(4,128)(2,1)}, bf16[4,512]{1,0:T(4,128)(2,1)}, bf16[4,512]{1,0:T(4,128)(2,1)}, f32[4,8]{1,0:T(4,128)}) custom-call(bf16[4,128]{1,0:T(4,128)(2,1)} %tokens_h.1, bf16[1,128]{1,0:T(2,128)(2,1)} %bitcast.9, bf16[512,512]{1,0:T(8,128)(2,1)} %wq_h.1, bf16[512,512]{1,0:T(8,128)(2,1)} %wk_h.1, bf16[512,512]{1,0:T(8,128)(2,1)} %wv_h.1, ...), custom_call_target="tpu_custom_call" | custom-call | tf_op jit(solution)/shard_map/pallas_call | solution.py:473
  41.5 1.3 %shard_map.175 = (bf16[4,128]{1,0:T(4,128)(2,1)}, bf16[4,512]{1,0:T(4,128)(2,1)}, bf16[4,512]{1,0:T(4,128)(2,1)}, f32[4,8]{1,0:T(4,128)}) custom-call(bf16[4,128]{1,0:T(4,128)(2,1)} %get-tuple-element.8.refs_0_, bf16[4,512]{1,0:T(4,128)(2,1)} %get-tuple-element.9.refs_1_, bf16[4,512]{1,0:T(4,128)(2,1)} %get-tuple-element.10.refs_2_, ...), custom_call_target="tpu_custom_call" | custom-call | tf_op jit(solution)/shard_map/pallas_call | solution.py:488

commit v3 on v2

--- a/solution.py
+++ b/solution.py
@@ -263,6 +263,9 @@
             sfx[b, :, cols] = whole[b * h : (b + 1) * h]
         carry = carry + (inside[:, 0:1] + chunk[:, 0:1])
 
+    for load in l_pk + l_pv + [l_fb, l_wo, l_wg, l_wu, l_wd]:
+        load.wait()
+
     from_kv(qmsg, sq, rq)
     total = qmsg[0]
     for n in range(1, nkv):
@@ -284,12 +287,10 @@
     lane = iota((h, LANES), 1)
     for b in range(B):
         spread_q = jnp.where(mine, jnp.broadcast_to(query[b : b + 1], (h, C)), 0.0).astype(BF16)
-        l_pk[b].wait()
         logits = across(spread_q, pk_v[b]) * scale + sfx[b]
         top = jnp.max(logits, axis=1, keepdims=True)
         weights = jnp.exp(logits - top)
         amount = jnp.sum(weights, axis=1, keepdims=True)
-        l_pv[b].wait()
         mixed = jnp.dot(weights.astype(BF16), pv_v[b], preferred_element_type=F32)
         mixbuf[b : b + 1, :] = jnp.sum(jnp.where(mine, mixed, 0.0), axis=0, keepdims=True)
         marks = (
@@ -316,7 +317,6 @@
     nv_ref[...] = new_values
     pre = finish(total[:, aux : aux + H], total[:, aux + H : aux + 2 * H])
     pick = (iota((H, LANES), 0) == iota((H, LANES), 1) + j * h).astype(F32)
-    l_fb.wait()
     gates = jnp.dot(pre, pick, precision=HIGHEST, preferred_element_type=F32)[:, 0:h] + fb_v[...]
     new_forget = jnp.minimum(gates, 0.0) - jnp.log1p(jnp.exp(-jnp.abs(gates)))
     nf_ref[...] = new_forget
@@ -329,7 +329,6 @@
         * scale
     )
     coef[...] = jnp.zeros(coef.shape, F32)
-    l_wo.wait()
 
     from_kv(astat, st, rt)
     tops, amounts = [None] * nkv, [None] * nkv
@@ -365,9 +364,6 @@
     to_kv(mmsg, sm, rm)
     for t in range(ntp):
         mpieces[t] = middle[:, t * c0 : (t + 1) * c0].astype(F32)
-    l_wg.wait()
-    l_wu.wait()
-    l_wd.wait()
     from_kv(mmsg, sm, rm)
     for n in range(nkv):
         mbuf[:, n * R : (n + 1) * R] = mmsg[n].astype(F32)

time: 43.1 us -> 42.1 us (0.977)
  Pallas kernels: 42.2 us -> 41.3 us
    pallas_call x1, Pallas kernels: 40.9 us -> 39.9 us  [local(): pl.pallas_call(functools.partial(kernel, nkv, ntp), out_shape=(jax.ShapeD...]
where the time goes in v3:
time: 42.1 us; the launch traced here: 41.9 us
  Pallas kernels  41.3 us (98%)
  between operations  0.65 us (2%)
    pallas_call x1, Pallas kernels, local(): pl.pallas_call(functools.partial(kernel, nkv, ntp), out_shape=(jax.ShapeD...  39.9 us
    pallas_call x1, Pallas kernels, local(): pl.pallas_call(hand_over, out_shape=tuple((jax.ShapeDtypeStruct(one.shape...  1.34 us

profile of v3, /device:TPU:0, one launch (start us, length us, event | category | flops | bytes accessed | tf_op | source)
XLA Modules:
  0.0 41.9 jit_solution(17346953794994709598)
XLA Ops:
  0.6 39.9 %shard_map.174 = (bf16[4,128]{1,0:T(4,128)(2,1)}, bf16[4,512]{1,0:T(4,128)(2,1)}, bf16[4,512]{1,0:T(4,128)(2,1)}, f32[4,8]{1,0:T(4,128)}) custom-call(bf16[4,128]{1,0:T(4,128)(2,1)} %tokens_h.1, bf16[1,128]{1,0:T(2,128)(2,1)} %bitcast.9, bf16[512,512]{1,0:T(8,128)(2,1)} %wq_h.1, bf16[512,512]{1,0:T(8,128)(2,1)} %wk_h.1, bf16[512,512]{1,0:T(8,128)(2,1)} %wv_h.1, ...), custom_call_target="tpu_custom_call" | custom-call | tf_op jit(solution)/shard_map/pallas_call | solution.py:469
  40.6 1.3 %shard_map.175 = (bf16[4,128]{1,0:T(4,128)(2,1)}, bf16[4,512]{1,0:T(4,128)(2,1)}, bf16[4,512]{1,0:T(4,128)(2,1)}, f32[4,8]{1,0:T(4,128)}) custom-call(bf16[4,128]{1,0:T(4,128)(2,1)} %get-tuple-element.8.refs_0_, bf16[4,512]{1,0:T(4,128)(2,1)} %get-tuple-element.9.refs_1_, bf16[4,512]{1,0:T(4,128)(2,1)} %get-tuple-element.10.refs_2_, ...), custom_call_target="tpu_custom_call" | custom-call | tf_op jit(solution)/shard_map/pallas_call | solution.py:484
